TPU v7x, 512 devices: a whole 4x8x8 slice. The times are simulated.
512 devices in a mesh: ep: 32 (over z, x), tp: 16 (over y, core).
Axes of the slice: x: 4, y: 8, z: 8, core: 2. Of those that a mesh axis runs over, the one named last changes fastest.
Arguments:
- tokens: bfloat16 [8192, 2048], P('ep')
- norm_gain: float32 [2048], replicated, may hold values from 0.1 to 1.9
- chosen: int32 [32, 1024], replicated, may hold values from 0 to 8191, as said below
- route_weight: float32 [32, 1024], P('ep'), may hold values from 0.2 to 1
- gate_weight: bfloat16 [32, 2048, 4096], P('ep', None, 'tp'), may hold values from -0.125 to 0.125
- up_weight: bfloat16 [32, 2048, 4096], P('ep', None, 'tp'), may hold values from -0.125 to 0.125
- down_weight: bfloat16 [32, 4096, 2048], P('ep', 'tp'), may hold values from -0.09375 to 0.09375
Outputs:
- combined: bfloat16 [8192, 2048], P('ep', 'tp')
Inputs may be any that keep to these rules, and one draw needn't show every extreme that they name: Each row of chosen lists 1024 distinct token numbers in ascending order. Of the 256 consecutive tokens of one index of ep, a row holds at most 48, and every draw has rows that hold exactly 48 of them.
All inputs are finite; a program needn't handle non-finite values.
Results may differ from a plain program's by a relative error of at most 0.02.
Values may be sent and summed in bfloat16 or wider, within the bound.
No kernel may reach another device: no remote copies, remote signals or barrier semaphores. Data moves between devices by JAX's collectives and lax.ppermute only.
A program may use at most 64 MiB of HBM per device.

v0:
```python
import jax
import jax.numpy as jnp
from jax import lax
from jax.sharding import Mesh
from jax.sharding import PartitionSpec as P

EP = ("ep_0", "ep_1")


def whole_of(x, axes, dim):
    if not axes:
        return x
    nearer = lax.all_gather(x, axes[-1], axis=dim, tiled=True)
    return whole_of(nearer, axes[:-1], dim)


def shards(tokens, norm_gain, chosen, route_weight, gate_weight, up_weight, down_weight):
    tok_rows, row_width = tokens.shape
    experts, capacity = chosen.shape
    ep_count = lax.axis_size(EP)
    tp_count = lax.axis_size("tp")
    owner_index = lax.axis_index(EP)
    lane_index = lax.axis_index("tp")
    slot_most = 3 * tok_rows // 16
    col_width = row_width // tp_count
    values = tokens.astype(jnp.float32)
    scale = lax.rsqrt(jnp.mean(values * values, axis=-1, keepdims=True) + 1e-06)
    normed = (values * scale * norm_gain[None, :]).astype(jnp.bfloat16)
    slot_steps = jnp.arange(slot_most, dtype=jnp.int32)
    first_token = owner_index * tok_rows
    run_start = jnp.sum((chosen < first_token).astype(jnp.int32), axis=1)
    run_end = jnp.sum((chosen < first_token + tok_rows).astype(jnp.int32), axis=1)
    run_count = run_end - run_start
    slot_live = slot_steps[None, :] < run_count[:, None]
    slot_place = jnp.minimum(run_start[:, None] + slot_steps[None, :], capacity - 1)
    slot_token = jnp.take_along_axis(chosen, slot_place, axis=1) - first_token
    my_chosen = lax.dynamic_index_in_dim(chosen, owner_index, 0, keepdims=False)
    block_edges = jnp.arange(ep_count, dtype=jnp.int32) * tok_rows
    src_start = jnp.sum((my_chosen[None, :] < block_edges[:, None]).astype(jnp.int32), axis=1)
    src_end = jnp.concatenate([src_start[1:], jnp.full((1,), capacity, jnp.int32)])
    gate_mat = gate_weight[0]
    up_mat = up_weight[0]
    down_mat = down_weight[0]
    my_columns = lax.dynamic_slice_in_dim(normed, lane_index * col_width, col_width, 1)
    all_columns = whole_of(my_columns, EP, 0)
    picked_rows = all_columns[my_chosen]
    segment = lax.all_gather(picked_rows, "tp", axis=1, tiled=True)
    gate_pre = jnp.dot(segment, gate_mat, preferred_element_type=jnp.float32)
    up_pre = jnp.dot(segment, up_mat, preferred_element_type=jnp.float32)
    hidden = (jax.nn.silu(gate_pre) * up_pre).astype(jnp.bfloat16)
    summed_out = lax.psum_scatter(
        lax.dot_general(
            down_mat, hidden, (((0,), (1,)), ((), ())), preferred_element_type=jnp.float32
        ).astype(jnp.bfloat16),
        "tp",
        scatter_dimension=0,
        tiled=True,
    ).astype(jnp.float32)
    weighted = (summed_out.T * route_weight[0][:, None]).astype(jnp.bfloat16)
    back_place = jnp.minimum(src_start[:, None] + slot_steps[None, :], capacity - 1)
    back_live = slot_steps[None, :] < (src_end - src_start)[:, None]
    outgoing_back = jnp.where(
        back_live[:, :, None], weighted[back_place], jnp.zeros((), jnp.bfloat16)
    )
    returned = lax.all_to_all(outgoing_back, EP, split_axis=0, concat_axis=0, tiled=True)
    target_row = jnp.where(slot_live, slot_token, tok_rows).reshape(-1)
    placement = (jnp.arange(tok_rows, dtype=jnp.int32)[:, None] == target_row[None, :]).astype(
        jnp.bfloat16
    )
    combined = jnp.dot(
        placement, returned.reshape(-1, col_width), preferred_element_type=jnp.float32
    )
    return combined.astype(jnp.bfloat16)


def solution(mesh):
    finer = Mesh(mesh.devices.reshape(8, 4, mesh.shape["tp"]), ("ep_0", "ep_1", "tp"))
    in_specs = (
        P(EP, None),
        P(),
        P(),
        P(EP, None),
        P(EP, None, "tp"),
        P(EP, None, "tp"),
        P(EP, "tp", None),
    )
    out_specs = P(EP, "tp")
    return jax.shard_map(
        shards, mesh=finer, in_specs=in_specs, out_specs=out_specs, check_vma=False
    )
```

profile of v0, /device:TPU:2, one launch (start us, length us, event | category | flops | bytes accessed | tf_op | source)
XLA Modules:
  0.0 248.5 jit_solution(2484285183497416496)
XLA Ops:
  6.5 0.0 copy-start
  6.5 0.0 copy-start.1
  6.5 0.0 all-gather.4.cloned.1.call-start
  6.5 1.5 convert_element_type.40
  8.1 1.5 multiply_reduce_fusion
  9.6 0.8 dynamic-slice
  10.4 0.1 fusion.17
  10.5 15.7 %all_gather.9 = bf16[1024,128]{1,0:T(8,128)(2,1)} all-gather(bf16[256,128]{1,0:T(8,128)(2,1)S(1)} %fusion.17), channel_id=1, replica_groups=mesh['ep_0'=8,'ep_1'=4,'tp'=16] {'ep_1'}, dimensions={0}, use_global_device_ids=true | all-gather | bytes 327680 | tf_op jit(solution)/shard_map/all_gather | solution.py:13
  26.2 0.0 all-gather.4.cloned.1.call-update
  26.2 0.0 all-gather.6.cloned.1.call-start
  26.2 0.0 copy-done.1
  26.3 46.0 %all-gather.4.cloned.1.call-done = bf16[8192,128]{1,0:T(8,128)(2,1)} async-done(((bf16[1024,128]{1,0:T(8,128)(2,1)}), bf16[8192,128]{1,0:T(8,128)(2,1)}) %all-gather.4.cloned.1.call-update) | async-done | bytes 2097168 | tf_op jit(solution)/shard_map/all_gather | solution.py:13
  72.3 5.9 %gather_fusion = bf16[1024,128]{1,0:T(8,128)(2,1)} fusion(bf16[8192,128]{1,0:T(8,128)(2,1)} %all-gather.4.cloned.1.call-done, s32[1024]{0:T(1024)S(1)} %broadcast_clamp_fusion), kind=kCustom, calls=%fused_computation | custom fusion | bytes 528384 | tf_op jit(solution)/shard_map/gather | solution.py:46
  78.2 0.0 copy-start.3
  78.2 0.0 all-gather.6.cloned.1.call-update
  78.2 0.0 reduce-scatter.4.cloned.1.call-start
  78.3 49.9 %all-gather.6.cloned.1.call-done = bf16[1024,2048]{1,0:T(8,128)(2,1)} async-done(((bf16[1024,128]{1,0:T(8,128)(2,1)}), bf16[1024,2048]{1,0:T(8,128)(2,1)}) %all-gather.6.cloned.1.call-update) | async-done | bytes 4194320 | tf_op jit(solution)/shard_map/all_gather | solution.py:47
  128.2 3.7 %fusion.6 = f32[1024,256]{1,0:T(8,128)S(1)} fusion(bf16[1024,2048]{1,0:T(8,128)(2,1)} %all-gather.6.cloned.1.call-done, bf16[1,2048,256]{2,1,0:T(8,128)(2,1)} %param.11), kind=kOutput, calls=%fused_computation.12 | convolution fusion | flops 1073741824 | bytes 6291456 | tf_op jit(solution)/shard_map/dot_general | solution.py:48
  132.0 0.0 copy-done
  132.0 0.0 copy-done.3
  132.0 8.5 %convert_bitcast_fusion = bf16[2048,1024]{0,1:T(8,128)(2,1)} fusion(bf16[1024,2048]{1,0:T(8,128)(2,1)} %all-gather.6.cloned.1.call-done, bf16[1,256,2048]{2,1,0:T(8,128)(2,1)S(1)} %copy-done, bf16[1,2048,256]{2,1,0:T(8,128)(2,1)S(1)} %copy-done.3, f32[1024,256]{1,0:T(8,128)S(1)} %fusion.6), kind=kOutput, calls=%fused_computation.3 | convolution fusion | flops 2151153664 | bytes 11534336 | tf_op jit(solution)/shard_map/dot_general | solution.py:52
  140.5 6.4 %copy.8 = bf16[2048,1024]{1,0:T(8,128)(2,1)} copy(bf16[2048,1024]{0,1:T(8,128)(2,1)} %convert_bitcast_fusion) | data formatting | bytes 8388608
  146.9 0.0 copy-start.2
  146.9 0.0 reduce-scatter.4.cloned.1.call-update
  146.9 0.2 convert_reduce_fusion
  147.1 0.1 slice.3
  147.2 0.1 compare_select_fusion
  147.3 0.1 reshape.234
  147.4 0.1 add_subtract_fusion
  147.4 0.1 iota_compare_fusion.4
  147.5 64.2 %reduce-scatter.4.cloned.1.call-done = bf16[128,1024]{1,0:T(8,128)(2,1)} async-done(((bf16[2048,1024]{1,0:T(8,128)(2,1)}), bf16[128,1024]{1,0:T(8,128)(2,1)}) %reduce-scatter.4.cloned.1.call-update) | async-done | bytes 262160
  211.7 1.1 copy.9
  212.8 0.0 copy-done.2
  212.8 0.2 fusion.15
  213.0 3.2 %gather_fusion.1 = bf16[1536,128]{1,0:T(8,128)(2,1)S(1)} fusion(bf16[1024,128]{1,0:T(8,128)(2,1)S(1)} %fusion.15, s32[2048]{0:T(1024)S(1)} %pad_clamp_fusion), kind=kCustom, calls=%fused_computation.1 | custom fusion | bytes 792576 | tf_op jit(solution)/shard_map/gather | solution.py:63
  216.2 1.0 broadcast_select_fusion
  217.3 10.3 %all-to-all-start = ((bf16[32,48,128]{2,1,0:T(8,128)(2,1)}), bf16[32,48,128]{2,1,0:T(8,128)(2,1)S(1)}, u32[]{:S(2)}, u32[]{:S(2)}) async-start(bf16[32,48,128]{2,1,0:T(8,128)(2,1)} %broadcast_select_fusion), calls=%async_computation | async-start | bytes 786432 | tf_op jit(solution)/shard_map/all_to_all | solution.py:65
  227.6 0.1 convert_reduce_fusion.1
  227.7 0.1 iota_compare_fusion.5
  227.8 0.1 lt.135
  227.9 0.1 fusion.20
  228.0 0.1 reshape.240
  228.1 12.6 %gather_fusion.2 = s32[1536]{0:T(1024)S(1)} fusion(s32[32,1024]{1,0:T(8,128)S(1)} %copy-done.1, s32[1536]{0:T(1024)S(1)} %reshape.240), kind=kCustom, calls=%fused_computation.2 | custom fusion | bytes 24576 | tf_op jit(solution)/shard_map/jit(take_along_axis)/gather | solution.py:36
  240.7 0.1 add.129
  240.7 0.1 add.130
  240.8 0.1 lt.137
  240.9 0.0 all-to-all-done
  240.9 1.0 fusion.2
  (8 shorter events, 0.1 us)
Async XLA Ops:
  6.5 125.4 %copy-start = (bf16[1,256,2048]{2,1,0:T(8,128)(2,1)S(1)}, bf16[1,256,2048]{2,1,0:T(8,128)(2,1)}, u32[]{:S(2)}) copy-start(bf16[1,256,2048]{2,1,0:T(8,128)(2,1)} %param.13) | copy-start | bytes 3145732
  6.5 19.7 %copy-start.1 = (s32[32,1024]{1,0:T(8,128)S(1)}, s32[32,1024]{1,0:T(8,128)}, u32[]{:S(2)}) copy-start(s32[32,1024]{1,0:T(8,128)} %param.9) | copy-start | bytes 393220
  6.5 65.7 %all-gather.4.cloned.1.call-start = ((), (), s32[]{:S(2)}) async-start(), calls=%async_computation.2 | async-start | bytes 2359296 | tf_op jit(solution)/shard_map/all_gather | solution.py:13
  26.2 102.0 %all-gather.6.cloned.1.call-start = ((), (), s32[]{:S(2)}) async-start(), calls=%async_computation.3 | async-start | bytes 4456448 | tf_op jit(solution)/shard_map/all_gather | solution.py:47
  78.2 53.8 %copy-start.3 = (bf16[1,2048,256]{2,1,0:T(8,128)(2,1)S(1)}, bf16[1,2048,256]{2,1,0:T(8,128)(2,1)}, u32[]{:S(2)}) copy-start(bf16[1,2048,256]{2,1,0:T(8,128)(2,1)} %param.12) | copy-start | bytes 3145732
  78.2 133.4 %reduce-scatter.4.cloned.1.call-start = ((), (), s32[]{:S(2)}) async-start(), calls=%async_computation.4 | async-start | bytes 4456448
  146.9 65.9 %copy-start.2 = (f32[1,1024]{1,0:T(1,128)S(1)}, f32[1,1024]{1,0:T(1,128)}, u32[]{:S(2)}) copy-start(f32[1,1024]{1,0:T(1,128)} %param.10) | copy-start | bytes 12292
  217.3 23.7 %all-to-all-start = ((bf16[32,48,128]{2,1,0:T(8,128)(2,1)}), bf16[32,48,128]{2,1,0:T(8,128)(2,1)S(1)}, u32[]{:S(2)}, u32[]{:S(2)}) async-start(bf16[32,48,128]{2,1,0:T(8,128)(2,1)} %broadcast_select_fusion), calls=%async_computation | async-start | bytes 786432 | tf_op jit(solution)/shard_map/all_to_all | solution.py:65
Sparse Core Ops, SparseCore 0:
  26.3 45.9 all-gather.3
  78.3 49.8 all-gather.5
  147.0 64.5 reduce-scatter.3
where the time goes:
time: 249 us; the launch traced here: 248 us
  waiting for transfers between devices  160 us (64%)
  local copies, waits for them, and re-layouts  30.6 us (12%)
  blocking collectives  15.7 us (6%)
  matrix products  13.3 us (5%)
  between operations  13.3 us (5%)
  starting transfers between devices  10.4 us (4%)
  other arithmetic  5.16 us (2%)
    unnamed x4, waiting for transfers between devices  64.2 us
    all_gather x1, waiting for transfers between devices, shards(): segment = lax.all_gather(picked_rows, 'tp', axis=1, tiled=True)  49.9 us
    all_gather x1, waiting for transfers between devices, whole_of(): nearer = lax.all_gather(x, axes[-1], axis=dim, tiled=True)  46 us
    all_gather x1, blocking collectives, whole_of(): nearer = lax.all_gather(x, axes[-1], axis=dim, tiled=True)  15.7 us
    gather x2, local copies, waits for them, and re-layouts, shards(): slot_token = jnp.take_along_axis(chosen, slot_place, axis=1) - first_token  12.7 us
    all_to_all x1, starting transfers between devices, shards(): lax.all_to_all(outgoing_back, EP, split_axis=0, concat_axis=0, tiled=True)  10.3 us
    dot_general x1, matrix products, shards(): lax.dot_general(down_mat, hidden, (((0,), (1,)), ((), ())), preferred_ele...  8.52 us
    unnamed x10, local copies, waits for them, and re-layouts  7.53 us
  transfers between devices with their start and end apart: 4, of which 3 were waited for; matrix products, arithmetic and copies ran while one was open for 6% of the time, Pallas kernels for 0%

commit v1 on v0

v1 whole, which is shorter than its diff:
```python
import jax
import jax.numpy as jnp
from jax import lax
from jax.sharding import Mesh
from jax.sharding import PartitionSpec as P

BF16 = jnp.bfloat16
F32 = jnp.float32


def shift(n, k):
    return [(i, (i + k) % n) for i in range(n)]


def dot(a, b, dims=(((1,), (0,)), ((), ()))):
    return lax.dot_general(a, b, dims, preferred_element_type=F32)


def shards(tokens, norm_gain, chosen, route_weight, gate_weight, up_weight, down_weight):
    tok_rows, width = tokens.shape
    experts, capacity = chosen.shape
    p = lax.axis_index("ep")
    y = lax.axis_index("y")
    c = lax.axis_index("c")
    q = y % 4
    h = y // 4
    block = width // 16
    quarter = width // 4
    half_rows = capacity // 2
    quart_rows = half_rows // 2
    slots = 3 * tok_rows // 32
    mate = [(0, 1), (1, 0)]

    def quarter_of(x, j, dim):
        shape = x.shape[:dim] + (2, 4, 2 * block) + x.shape[dim + 1 :]
        picked = lax.dynamic_index_in_dim(x.reshape(shape), j % 4, dim + 1, keepdims=False)
        return picked.reshape(x.shape[:dim] + (quarter,) + x.shape[dim + 1 :])

    first_token = p * tok_rows
    run_start = jnp.sum((chosen < first_token).astype(jnp.int32), axis=1)
    run_end = jnp.sum((chosen < first_token + tok_rows).astype(jnp.int32), axis=1)
    first = run_start + ((run_start + c) % 2)
    slot_rank = first[:, None] + 2 * jnp.arange(slots, dtype=jnp.int32)[None, :]
    rank = jnp.arange(capacity, dtype=jnp.int32)
    slot_token = jnp.sum(
        jnp.where(rank[None, None, :] == slot_rank[:, :, None], chosen[:, None, :], 0), axis=2
    )
    slot_local = jnp.where(slot_rank < run_end[:, None], slot_token - first_token, tok_rows)
    pick_token = (
        slot_local[:, :, None] == jnp.arange(tok_rows, dtype=jnp.int32)[None, None, :]
    ).astype(BF16).reshape(experts * slots, tok_rows)

    mine = lax.dynamic_index_in_dim(chosen, p, 0, keepdims=False)
    edges = jnp.arange(experts + 1, dtype=jnp.int32) * tok_rows
    src_edge = jnp.sum((mine[None, :] < edges[:, None]).astype(jnp.int32), axis=1)
    k_edge = (src_edge - c + 1) // 2
    k_slot = k_edge[:-1, None] + jnp.arange(slots, dtype=jnp.int32)[None, :]
    k_slot = jnp.where(k_slot < k_edge[1:, None], k_slot, half_rows)
    pick_row = (
        k_slot[:, :, None] == jnp.arange(half_rows, dtype=jnp.int32)[None, None, :]
    ).astype(BF16).reshape(experts * slots, half_rows)
    my_weight = lax.dynamic_index_in_dim(
        route_weight.reshape(half_rows, 2), c, 1, keepdims=True
    )

    values = tokens.astype(F32)
    scale = lax.rsqrt(jnp.mean(values * values, axis=-1, keepdims=True) + 1e-06)
    my_gain = quarter_of(norm_gain, q, 0)
    normed = (quarter_of(tokens, q, 1).astype(F32) * scale * my_gain[None, :]).astype(BF16)

    sent = dot(pick_token, normed).astype(BF16).reshape(experts, slots, quarter)
    got = lax.all_to_all(sent, "ep", 0, 0, tiled=True).reshape(experts * slots, quarter)
    own = dot(pick_row, got, (((0,), (0,)), ((), ()))).astype(BF16)

    def around(x_up, x_down, x_up2, x_down2):
        return (
            lax.ppermute(x_up, "y", shift(8, 1)),
            lax.ppermute(x_down, "y", shift(8, -1)),
            lax.ppermute(x_up2, "y", shift(8, 2)),
            lax.ppermute(x_down2, "y", shift(8, -2)),
        )

    below, above, far_a, far_b = around(own, own, own[:quart_rows], own[quart_rows:])
    far = jnp.concatenate([far_a, far_b], axis=0)

    gate_w, up_w, down_w = gate_weight[0], up_weight[0], down_weight[0]
    gate_w, up_w, down_w, own = lax.optimization_barrier((gate_w, up_w, down_w, own))
    gate_m = lax.ppermute(gate_w, "c", mate)
    up_m = lax.ppermute(up_w, "c", mate)
    down_m = lax.ppermute(down_w, "c", mate)

    def hidden_of(gate_mat, up_mat):
        pre = [
            sum(dot(x, quarter_of(w, q + j, 0)) for x, j in ((own, 0), (below, 3), (above, 1), (far, 2)))
            for w in (gate_mat, up_mat)
        ]
        return (jax.nn.silu(pre[0]) * pre[1]).astype(BF16)

    hid = hidden_of(gate_w, up_w)
    hid_m = hidden_of(gate_m, up_m)

    def out_of(j):
        return dot(hid, quarter_of(down_w, q + j, 1)) + dot(hid_m, quarter_of(down_m, q + j, 1))

    out_far = out_of(2).astype(BF16)
    r_below, r_above, r_far_a, r_far_b = around(
        out_of(1).astype(BF16), out_of(3).astype(BF16), out_far[:quart_rows], out_far[quart_rows:]
    )
    total = out_of(0) + r_below.astype(F32) + r_above.astype(F32)
    total = total + jnp.concatenate([r_far_a, r_far_b], axis=0).astype(F32)
    weighted = (my_weight * total).astype(BF16)

    back = dot(pick_row, weighted).astype(BF16).reshape(experts, slots, quarter)
    returned = lax.all_to_all(back, "ep", 0, 0, tiled=True).reshape(experts * slots, quarter)
    part = dot(pick_token, returned, (((0,), (0,)), ((), ()))).reshape(tok_rows, 2, 2, block)

    def cell(i, j):
        row = lax.dynamic_index_in_dim(part, i % 2, 1, keepdims=False)
        return lax.dynamic_index_in_dim(row, j % 2, 1, keepdims=False)

    opposite = shift(8, 4)
    both = [((i, j), ((i + 4) % 8, 1 - j)) for i in range(8) for j in range(2)]
    both = [(2 * a + b, 2 * d + e) for (a, b), (d, e) in both]
    from_mate = lax.ppermute(cell(h, c + 1).astype(BF16), "c", mate)
    from_far = lax.ppermute(cell(h + 1, c).astype(BF16), "y", opposite)
    from_both = lax.ppermute(cell(h + 1, c + 1).astype(BF16), ("y", "c"), both)
    combined = cell(h, c) + from_mate.astype(F32) + from_far.astype(F32) + from_both.astype(F32)
    return combined.astype(BF16)


def solution(mesh):
    finer = Mesh(mesh.devices.reshape(mesh.shape["ep"], 8, 2), ("ep", "y", "c"))
    tp = ("y", "c")
    in_specs = (
        P("ep", None),
        P(),
        P(),
        P("ep", None),
        P("ep", None, tp),
        P("ep", None, tp),
        P("ep", tp, None),
    )
    return jax.shard_map(
        shards, mesh=finer, in_specs=in_specs, out_specs=P("ep", tp), check_vma=False
    )
```

time: 249 us -> 163 us (0.65)
  the two profiles are of different devices: /device:TPU:2 before, /device:TPU:11 now
where the time goes in v1:
time: 163 us; the launch traced here: 162 us
  starting transfers between devices  75.2 us (46%)
  waiting for transfers between devices  63.9 us (39%)
  matrix products  11.6 us (7%)
  local copies, waits for them, and re-layouts  5.89 us (4%)
  other arithmetic  4.94 us (3%)
    all_to_all x1, waiting for transfers between devices, shards(): lax.all_to_all(back, 'ep', 0, 0, tiled=True)  20.3 us
    all_to_all x1, waiting for transfers between devices, shards(): lax.all_to_all(sent, 'ep', 0, 0, tiled=True)  18.4 us
    ppermute x2, waiting for transfers between devices, around(): lax.ppermute(x_down2, 'y', shift(8, -2))  15.3 us
    all_to_all x1, starting transfers between devices, shards(): lax.all_to_all(sent, 'ep', 0, 0, tiled=True)  13 us
    dot_general x27, matrix products, dot(): return lax.dot_general(a, b, dims, preferred_element_type=F32)  11.6 us
    ppermute x1, starting transfers between devices, shards(): from_both = lax.ppermute(cell(h + 1, c + 1).astype(BF16), ('y', 'c'), both)  9.59 us
    ppermute x2, starting transfers between devices, around(): lax.ppermute(x_up2, 'y', shift(8, 2))  9.01 us
    ppermute x2, starting transfers between devices, around(): lax.ppermute(x_up, 'y', shift(8, 1))  8.81 us
  transfers between devices with their start and end apart: 16, of which 6 were waited for; matrix products, arithmetic and copies ran while one was open for 5% of the time, Pallas kernels for 0%

profile of v1, /device:TPU:11, one launch (start us, length us, event | category | flops | bytes accessed | tf_op | source)
XLA Modules:
  0.0 162.3 jit_solution(13460874859983938823)
XLA Ops:
  0.0 1.9 %reshape.319 = bf16[256,2,4,256]{3,2,1,0:T(4,128)(2,1)S(1)} reshape(bf16[256,2048]{1,0:T(8,128)(2,1)} %param.7) | data formatting | bytes 2097152 | tf_op jit(solution)/shard_map/reshape | solution.py:36
  2.3 0.6 copy-done.4
  3.1 1.0 select_reduce_fusion
  4.7 1.8 %convert_reduce_fusion = f32[256,2,256]{2,1,0:T(2,128)S(1)} fusion(bf16[256,2,4,256]{3,2,1,0:T(4,128)(2,1)S(1)} %reshape.319, s32[]{:T(128)S(6)} %select_n.213), kind=kLoop, calls=%fused_computation.47 | loop fusion | flops 131072 | bytes 786436 | tf_op jit(solution)/shard_map/convert_element_type | solution.py:69
  6.6 1.4 convolution_convert_fusion
  7.9 13.0 %all-to-all-start = ((bf16[32,24,512]{2,1,0:T(8,128)(2,1)}), bf16[32,24,512]{2,1,0:T(8,128)(2,1)S(1)}, u32[]{:S(2)}, u32[]{:S(2)}) async-start(bf16[32,24,512]{2,1,0:T(8,128)(2,1)} %bitcast.7), calls=%async_computation | async-start | bytes 1572864 | tf_op jit(solution)/shard_map/all_to_all | solution.py:72
  21.5 0.5 copy.21
  22.3 0.5 broadcast.179
  22.8 0.7 reduce.7
  23.9 18.4 %all-to-all-done = bf16[32,24,512]{2,1,0:T(8,128)(2,1)S(1)} async-done(((bf16[32,24,512]{2,1,0:T(8,128)(2,1)}), bf16[32,24,512]{2,1,0:T(8,128)(2,1)S(1)}, u32[]{:S(2)}, u32[]{:S(2)}) %all-to-all-start) | async-done | bytes 786464 | tf_op jit(solution)/shard_map/all_to_all | solution.py:72
  42.4 0.8 fusion.8
  43.2 3.3 %collective-permute-start = (bf16[512,512]{1,0:T(8,128)(2,1)S(1)}, bf16[512,512]{1,0:T(8,128)(2,1)S(1)}, u32[]{:S(2)}, u32[]{:S(2)}) collective-permute-start(bf16[512,512]{1,0:T(8,128)(2,1)S(1)} %fusion.8), channel_id=1, source_target_pairs={{0,2},{2,4},{4,6},{6,8},{8,10},{10,12},{12,14},{14,0},{1,3},{3,5},... | collective-permute-start | bytes 1572872 | tf_op jit(solution)/shard_map/ppermute | solution.py:77
  46.6 2.1 %collective-permute-start.1 = (bf16[512,512]{1,0:T(8,128)(2,1)S(1)}, bf16[512,512]{1,0:T(8,128)(2,1)S(1)}, u32[]{:S(2)}, u32[]{:S(2)}) collective-permute-start(bf16[512,512]{1,0:T(8,128)(2,1)S(1)} %fusion.8), channel_id=1, source_target_pairs={{0,14},{2,0},{4,2},{6,4},{8,6},{10,8},{12,10},{14,12},{1,15},{3,1}... | collective-permute-start | bytes 1572872 | tf_op jit(solution)/shard_map/ppermute | solution.py:78
  48.7 5.3 %collective-permute-start.2 = (bf16[256,512]{1,0:T(8,128)(2,1)S(1)}, bf16[256,512]{1,0:T(8,128)(2,1)S(1)}, u32[]{:S(2)}, u32[]{:S(2)}) collective-permute-start(bf16[256,512]{1,0:T(8,128)(2,1)S(1)} %get-tuple-element.45), channel_id=1, source_target_pairs={{0,4},{2,6},{4,8},{6,10},{8,12},{10,14},{12,0},{14,2},{1,5},{3,7},... | collective-permute-start | bytes 786440 | tf_op jit(solution)/shard_map/ppermute | solution.py:79
  54.0 2.1 %collective-permute-start.3 = (bf16[256,512]{1,0:T(8,128)(2,1)S(1)}, bf16[256,512]{1,0:T(8,128)(2,1)S(1)}, u32[]{:S(2)}, u32[]{:S(2)}) collective-permute-start(bf16[256,512]{1,0:T(8,128)(2,1)S(1)} %get-tuple-element.44), channel_id=1, source_target_pairs={{0,12},{2,14},{4,0},{6,2},{8,4},{10,6},{12,8},{14,10},{1,13},{3,15... | collective-permute-start | bytes 786440 | tf_op jit(solution)/shard_map/ppermute | solution.py:80
  56.1 5.3 %collective-permute-start.5 = (bf16[2048,256]{1,0:T(8,128)(2,1)S(1)}, bf16[2048,256]{1,0:T(8,128)(2,1)S(1)}, u32[]{:S(2)}, u32[]{:S(2)}) collective-permute-start(bf16[2048,256]{1,0:T(8,128)(2,1)S(1)} %bitcast.130), channel_id=1, source_target_pairs={{0,1},{1,0},{2,3},{3,2},{4,5},{5,4},{6,7},{7,6},{8,9},{9,8},{10,11... | collective-permute-start | bytes 3145736 | tf_op jit(solution)/shard_map/ppermute | solution.py:89
  62.3 4.3 %collective-permute-done.2 = bf16[256,512]{1,0:T(8,128)(2,1)S(1)} collective-permute-done((bf16[256,512]{1,0:T(8,128)(2,1)S(1)}, bf16[256,512]{1,0:T(8,128)(2,1)S(1)}, u32[]{:S(2)}, u32[]{:S(2)}) %collective-permute-start.2) | collective-permute-done | bytes 262176 | tf_op jit(solution)/shard_map/ppermute | solution.py:79
  66.6 7.8 %collective-permute-start.4 = (bf16[2048,256]{1,0:T(8,128)(2,1)S(1)}, bf16[2048,256]{1,0:T(8,128)(2,1)S(1)}, u32[]{:S(2)}, u32[]{:S(2)}) collective-permute-start(bf16[2048,256]{1,0:T(8,128)(2,1)S(1)} %bitcast.133), channel_id=1, source_target_pairs={{0,1},{1,0},{2,3},{3,2},{4,5},{5,4},{6,7},{7,6},{8,9},{9,8},{10,11... | collective-permute-start | bytes 3145736 | tf_op jit(solution)/shard_map/ppermute | solution.py:88
  74.4 2.1 %collective-permute-start.6 = (bf16[256,2048]{0,1:T(8,128)(2,1)S(1)}, bf16[256,2048]{0,1:T(8,128)(2,1)S(1)}, u32[]{:S(2)}, u32[]{:S(2)}) collective-permute-start(bf16[256,2048]{0,1:T(8,128)(2,1)S(1)} %bitcast.118), channel_id=1, source_target_pairs={{0,1},{1,0},{2,3},{3,2},{4,5},{5,4},{6,7},{7,6},{8,9},{9,8},{10,11... | collective-permute-start | bytes 3145736 | tf_op jit(solution)/shard_map/ppermute | solution.py:90
  76.5 0.3 fusion.50
  77.5 0.3 convolution_add_fusion.7
  77.8 0.3 fusion.18
  78.1 0.3 multiply_convert_fusion.1
  78.4 0.3 fusion.61
  78.7 0.3 fusion.60
  79.1 0.3 fusion.62
  80.6 0.3 fusion.54
  80.9 0.3 fusion.16
  81.8 0.3 multiply_convert_fusion
  82.2 0.3 fusion.10
  82.5 2.7 %collective-permute-start.8 = (bf16[512,512]{1,0:T(8,128)(2,1)S(1)}, bf16[512,512]{1,0:T(8,128)(2,1)S(1)}, u32[]{:S(2)}, u32[]{:S(2)}) collective-permute-start(bf16[512,512]{1,0:T(8,128)(2,1)S(1)} %fusion.10), channel_id=1, source_target_pairs={{0,14},{2,0},{4,2},{6,4},{8,6},{10,8},{12,10},{14,12},{1,15},{3,1}... | collective-permute-start | bytes 1572872 | tf_op jit(solution)/shard_map/ppermute | solution.py:78
  85.2 0.3 fusion.9
  85.6 5.5 %collective-permute-start.7 = (bf16[512,512]{1,0:T(8,128)(2,1)S(1)}, bf16[512,512]{1,0:T(8,128)(2,1)S(1)}, u32[]{:S(2)}, u32[]{:S(2)}) collective-permute-start(bf16[512,512]{1,0:T(8,128)(2,1)S(1)} %fusion.9), channel_id=1, source_target_pairs={{0,2},{2,4},{4,6},{6,8},{8,10},{10,12},{12,14},{14,0},{1,3},{3,5},... | collective-permute-start | bytes 1572872 | tf_op jit(solution)/shard_map/ppermute | solution.py:77
  91.0 0.3 fusion.11
  91.4 2.5 %collective-permute-start.10 = (bf16[256,512]{1,0:T(8,128)(2,1)S(1)}, bf16[256,512]{1,0:T(8,128)(2,1)S(1)}, u32[]{:S(2)}, u32[]{:S(2)}) collective-permute-start(bf16[256,512]{1,0:T(8,128)(2,1)S(1)} %get-tuple-element.43), channel_id=1, source_target_pairs={{0,12},{2,14},{4,0},{6,2},{8,4},{10,6},{12,8},{14,10},{1,13},{3,15... | collective-permute-start | bytes 786440 | tf_op jit(solution)/shard_map/ppermute | solution.py:80
  93.9 3.7 %collective-permute-start.9 = (bf16[256,512]{1,0:T(8,128)(2,1)S(1)}, bf16[256,512]{1,0:T(8,128)(2,1)S(1)}, u32[]{:S(2)}, u32[]{:S(2)}) collective-permute-start(bf16[256,512]{1,0:T(8,128)(2,1)S(1)} %get-tuple-element.42), channel_id=1, source_target_pairs={{0,4},{2,6},{4,8},{6,10},{8,12},{10,14},{12,0},{14,2},{1,5},{3,7},... | collective-permute-start | bytes 786440 | tf_op jit(solution)/shard_map/ppermute | solution.py:79
  97.6 0.3 fusion.53
  98.0 15.3 %collective-permute-done.10 = bf16[256,512]{1,0:T(8,128)(2,1)S(1)} collective-permute-done((bf16[256,512]{1,0:T(8,128)(2,1)S(1)}, bf16[256,512]{1,0:T(8,128)(2,1)S(1)}, u32[]{:S(2)}, u32[]{:S(2)}) %collective-permute-start.10) | collective-permute-done | bytes 262176 | tf_op jit(solution)/shard_map/ppermute | solution.py:80
  113.2 0.8 collective-permute-done.9
  114.1 1.9 %fusion.2 = bf16[768,512]{1,0:T(8,128)(2,1)} fusion(f32[512,512]{1,0:T(8,128)S(1)} %fusion.53, bf16[512,256]{1,0:T(8,128)(2,1)S(1)} %multiply_convert_fusion, bf16[256,512]{0,1:T(8,128)(2,1)S(1)} %bitcast.151, bf16[512,512]{1,0:T(8,128)(2,1)S(1)} %collective-permute-done.8, bf16[512,512]{1,0:T(8,128)(2,1)S(1)} %collective-permute-done.7, ...), kind=kOutput, calls=%fused_computation.7 | convolution fusion | flops 540803072 | bytes 3937280 | tf_op jit(solution)/shard_map/dot_general | solution.py:16
  115.9 5.5 %all-to-all-start.1 = ((bf16[32,24,512]{2,1,0:T(8,128)(2,1)}), bf16[32,24,512]{2,1,0:T(8,128)(2,1)S(1)}, u32[]{:S(2)}, u32[]{:S(2)}) async-start(bf16[32,24,512]{2,1,0:T(8,128)(2,1)} %bitcast.39), calls=%async_computation.1 | async-start | bytes 1572864 | tf_op jit(solution)/shard_map/all_to_all | solution.py:114
  121.5 20.3 %all-to-all-done.1 = bf16[32,24,512]{2,1,0:T(8,128)(2,1)S(1)} async-done(((bf16[32,24,512]{2,1,0:T(8,128)(2,1)}), bf16[32,24,512]{2,1,0:T(8,128)(2,1)S(1)}, u32[]{:S(2)}, u32[]{:S(2)}) %all-to-all-start.1) | async-done | bytes 786464 | tf_op jit(solution)/shard_map/all_to_all | solution.py:114
  142.0 0.4 fusion.26
  142.5 9.6 %collective-permute-start.13 = (bf16[256,128]{1,0:T(8,128)(2,1)S(1)}, bf16[256,128]{1,0:T(8,128)(2,1)S(1)}, u32[]{:S(2)}, u32[]{:S(2)}) collective-permute-start(bf16[256,128]{1,0:T(8,128)(2,1)S(1)} %get-tuple-element.40), channel_id=1, source_target_pairs={{0,9},{1,8},{2,11},{3,10},{4,13},{5,12},{6,15},{7,14},{8,1},{9,0},... | collective-permute-start | bytes 196616 | tf_op jit(solution)/shard_map/ppermute | solution.py:126
  152.1 2.8 %collective-permute-start.12 = (bf16[256,128]{1,0:T(8,128)(2,1)S(1)}, bf16[256,128]{1,0:T(8,128)(2,1)S(1)}, u32[]{:S(2)}, u32[]{:S(2)}) collective-permute-start(bf16[256,128]{1,0:T(8,128)(2,1)S(1)} %get-tuple-element.41), channel_id=1, source_target_pairs={{0,8},{2,10},{4,12},{6,14},{8,0},{10,2},{12,4},{14,6},{1,9},{3,11}... | collective-permute-start | bytes 196616 | tf_op jit(solution)/shard_map/ppermute | solution.py:125
  154.9 1.9 %collective-permute-start.11 = (bf16[256,128]{1,0:T(8,128)(2,1)S(1)}, bf16[256,128]{1,0:T(8,128)(2,1)S(1)}, u32[]{:S(2)}, u32[]{:S(2)}) collective-permute-start(bf16[256,128]{1,0:T(8,128)(2,1)S(1)} %get-tuple-element.39), channel_id=1, source_target_pairs={{0,1},{1,0},{2,3},{3,2},{4,5},{5,4},{6,7},{7,6},{8,9},{9,8},{10,11... | collective-permute-start | bytes 196616 | tf_op jit(solution)/shard_map/ppermute | solution.py:124
  156.9 4.8 %collective-permute-done.12 = bf16[256,128]{1,0:T(8,128)(2,1)S(1)} collective-permute-done((bf16[256,128]{1,0:T(8,128)(2,1)S(1)}, bf16[256,128]{1,0:T(8,128)(2,1)S(1)}, u32[]{:S(2)}, u32[]{:S(2)}) %collective-permute-start.12) | collective-permute-done | bytes 65568 | tf_op jit(solution)/shard_map/ppermute | solution.py:125
  161.7 0.7 fusion.38
  (74 shorter events, 5.8 us)
Async XLA Ops:
  0.0 1.9 %copy-start = (bf16[256,2048]{1,0:T(8,128)(2,1)S(1)}, bf16[256,2048]{1,0:T(8,128)(2,1)}, u32[]{:S(2)}) copy-start(bf16[256,2048]{1,0:T(8,128)(2,1)} %param.7) | copy-start | bytes 3145732
  2.0 0.9 copy-start.4
  4.7 1.8 %copy-start.5 = (f32[2048]{0:T(1024)S(1)}, f32[2048]{0:T(1024)}, u32[]{:S(2)}) copy-start(f32[2048]{0:T(1024)} %param.8) | copy-start | bytes 24580
  7.9 13.6 %copy-start.3 = (bf16[1,256,2048]{2,1,0:T(8,128)(2,1)S(1)}, bf16[1,256,2048]{2,1,0:T(8,128)(2,1)}, u32[]{:S(2)}) copy-start(bf16[1,256,2048]{2,1,0:T(8,128)(2,1)} %param.13) | copy-start | bytes 3145732
  7.9 34.4 %all-to-all-start = ((bf16[32,24,512]{2,1,0:T(8,128)(2,1)}), bf16[32,24,512]{2,1,0:T(8,128)(2,1)S(1)}, u32[]{:S(2)}, u32[]{:S(2)}) async-start(bf16[32,24,512]{2,1,0:T(8,128)(2,1)} %bitcast.7), calls=%async_computation | async-start | bytes 1572864 | tf_op jit(solution)/shard_map/all_to_all | solution.py:72
  21.5 1.3 copy-start.6
  42.4 19.0 %copy-start.2 = (bf16[1,2048,256]{2,1,0:T(8,128)(2,1)S(1)}, bf16[1,2048,256]{2,1,0:T(8,128)(2,1)}, u32[]{:S(2)}) copy-start(bf16[1,2048,256]{2,1,0:T(8,128)(2,1)} %param.11) | copy-start | bytes 3145732
  43.2 12.9 %copy-start.1 = (bf16[1,2048,256]{2,1,0:T(8,128)(2,1)S(1)}, bf16[1,2048,256]{2,1,0:T(8,128)(2,1)}, u32[]{:S(2)}) copy-start(bf16[1,2048,256]{2,1,0:T(8,128)(2,1)} %param.12) | copy-start | bytes 3145732
  43.2 33.9 %collective-permute-start = (bf16[512,512]{1,0:T(8,128)(2,1)S(1)}, bf16[512,512]{1,0:T(8,128)(2,1)S(1)}, u32[]{:S(2)}, u32[]{:S(2)}) collective-permute-start(bf16[512,512]{1,0:T(8,128)(2,1)S(1)} %fusion.8), channel_id=1, source_target_pairs={{0,2},{2,4},{4,6},{6,8},{8,10},{10,12},{12,14},{14,0},{1,3},{3,5},... | collective-permute-start | bytes 1572872 | tf_op jit(solution)/shard_map/ppermute | solution.py:77
  46.6 31.2 %collective-permute-start.1 = (bf16[512,512]{1,0:T(8,128)(2,1)S(1)}, bf16[512,512]{1,0:T(8,128)(2,1)S(1)}, u32[]{:S(2)}, u32[]{:S(2)}) collective-permute-start(bf16[512,512]{1,0:T(8,128)(2,1)S(1)} %fusion.8), channel_id=1, source_target_pairs={{0,14},{2,0},{4,2},{6,4},{8,6},{10,8},{12,10},{14,12},{1,15},{3,1}... | collective-permute-start | bytes 1572872 | tf_op jit(solution)/shard_map/ppermute | solution.py:78
  48.7 17.9 %collective-permute-start.2 = (bf16[256,512]{1,0:T(8,128)(2,1)S(1)}, bf16[256,512]{1,0:T(8,128)(2,1)S(1)}, u32[]{:S(2)}, u32[]{:S(2)}) collective-permute-start(bf16[256,512]{1,0:T(8,128)(2,1)S(1)} %get-tuple-element.45), channel_id=1, source_target_pairs={{0,4},{2,6},{4,8},{6,10},{8,12},{10,14},{12,0},{14,2},{1,5},{3,7},... | collective-permute-start | bytes 786440 | tf_op jit(solution)/shard_map/ppermute | solution.py:79
  54.0 20.4 %collective-permute-start.3 = (bf16[256,512]{1,0:T(8,128)(2,1)S(1)}, bf16[256,512]{1,0:T(8,128)(2,1)S(1)}, u32[]{:S(2)}, u32[]{:S(2)}) collective-permute-start(bf16[256,512]{1,0:T(8,128)(2,1)S(1)} %get-tuple-element.44), channel_id=1, source_target_pairs={{0,12},{2,14},{4,0},{6,2},{8,4},{10,6},{12,8},{14,10},{1,13},{3,15... | collective-permute-start | bytes 786440 | tf_op jit(solution)/shard_map/ppermute | solution.py:80
  56.1 23.3 %collective-permute-start.5 = (bf16[2048,256]{1,0:T(8,128)(2,1)S(1)}, bf16[2048,256]{1,0:T(8,128)(2,1)S(1)}, u32[]{:S(2)}, u32[]{:S(2)}) collective-permute-start(bf16[2048,256]{1,0:T(8,128)(2,1)S(1)} %bitcast.130), channel_id=1, source_target_pairs={{0,1},{1,0},{2,3},{3,2},{4,5},{5,4},{6,7},{7,6},{8,9},{9,8},{10,11... | collective-permute-start | bytes 3145736 | tf_op jit(solution)/shard_map/ppermute | solution.py:89
  66.6 12.8 %collective-permute-start.4 = (bf16[2048,256]{1,0:T(8,128)(2,1)S(1)}, bf16[2048,256]{1,0:T(8,128)(2,1)S(1)}, u32[]{:S(2)}, u32[]{:S(2)}) collective-permute-start(bf16[2048,256]{1,0:T(8,128)(2,1)S(1)} %bitcast.133), channel_id=1, source_target_pairs={{0,1},{1,0},{2,3},{3,2},{4,5},{5,4},{6,7},{7,6},{8,9},{9,8},{10,11... | collective-permute-start | bytes 3145736 | tf_op jit(solution)/shard_map/ppermute | solution.py:88
  74.4 5.8 %collective-permute-start.6 = (bf16[256,2048]{0,1:T(8,128)(2,1)S(1)}, bf16[256,2048]{0,1:T(8,128)(2,1)S(1)}, u32[]{:S(2)}, u32[]{:S(2)}) collective-permute-start(bf16[256,2048]{0,1:T(8,128)(2,1)S(1)} %bitcast.118), channel_id=1, source_target_pairs={{0,1},{1,0},{2,3},{3,2},{4,5},{5,4},{6,7},{7,6},{8,9},{9,8},{10,11... | collective-permute-start | bytes 3145736 | tf_op jit(solution)/shard_map/ppermute | solution.py:90
  82.5 31.5 %collective-permute-start.8 = (bf16[512,512]{1,0:T(8,128)(2,1)S(1)}, bf16[512,512]{1,0:T(8,128)(2,1)S(1)}, u32[]{:S(2)}, u32[]{:S(2)}) collective-permute-start(bf16[512,512]{1,0:T(8,128)(2,1)S(1)} %fusion.10), channel_id=1, source_target_pairs={{0,14},{2,0},{4,2},{6,4},{8,6},{10,8},{12,10},{14,12},{1,15},{3,1}... | collective-permute-start | bytes 1572872 | tf_op jit(solution)/shard_map/ppermute | solution.py:78
  85.6 28.5 %collective-permute-start.7 = (bf16[512,512]{1,0:T(8,128)(2,1)S(1)}, bf16[512,512]{1,0:T(8,128)(2,1)S(1)}, u32[]{:S(2)}, u32[]{:S(2)}) collective-permute-start(bf16[512,512]{1,0:T(8,128)(2,1)S(1)} %fusion.9), channel_id=1, source_target_pairs={{0,2},{2,4},{4,6},{6,8},{8,10},{10,12},{12,14},{14,0},{1,3},{3,5},... | collective-permute-start | bytes 1572872 | tf_op jit(solution)/shard_map/ppermute | solution.py:77
  91.4 21.8 %collective-permute-start.10 = (bf16[256,512]{1,0:T(8,128)(2,1)S(1)}, bf16[256,512]{1,0:T(8,128)(2,1)S(1)}, u32[]{:S(2)}, u32[]{:S(2)}) collective-permute-start(bf16[256,512]{1,0:T(8,128)(2,1)S(1)} %get-tuple-element.43), channel_id=1, source_target_pairs={{0,12},{2,14},{4,0},{6,2},{8,4},{10,6},{12,8},{14,10},{1,13},{3,15... | collective-permute-start | bytes 786440 | tf_op jit(solution)/shard_map/ppermute | solution.py:80
  93.9 20.2 %collective-permute-start.9 = (bf16[256,512]{1,0:T(8,128)(2,1)S(1)}, bf16[256,512]{1,0:T(8,128)(2,1)S(1)}, u32[]{:S(2)}, u32[]{:S(2)}) collective-permute-start(bf16[256,512]{1,0:T(8,128)(2,1)S(1)} %get-tuple-element.42), channel_id=1, source_target_pairs={{0,4},{2,6},{4,8},{6,10},{8,12},{10,14},{12,0},{14,2},{1,5},{3,7},... | collective-permute-start | bytes 786440 | tf_op jit(solution)/shard_map/ppermute | solution.py:79
  115.9 25.8 %all-to-all-start.1 = ((bf16[32,24,512]{2,1,0:T(8,128)(2,1)}), bf16[32,24,512]{2,1,0:T(8,128)(2,1)S(1)}, u32[]{:S(2)}, u32[]{:S(2)}) async-start(bf16[32,24,512]{2,1,0:T(8,128)(2,1)} %bitcast.39), calls=%async_computation.1 | async-start | bytes 1572864 | tf_op jit(solution)/shard_map/all_to_all | solution.py:114
  142.5 14.4 %collective-permute-start.13 = (bf16[256,128]{1,0:T(8,128)(2,1)S(1)}, bf16[256,128]{1,0:T(8,128)(2,1)S(1)}, u32[]{:S(2)}, u32[]{:S(2)}) collective-permute-start(bf16[256,128]{1,0:T(8,128)(2,1)S(1)} %get-tuple-element.40), channel_id=1, source_target_pairs={{0,9},{1,8},{2,11},{3,10},{4,13},{5,12},{6,15},{7,14},{8,1},{9,0},... | collective-permute-start | bytes 196616 | tf_op jit(solution)/shard_map/ppermute | solution.py:126
  152.1 9.5 %collective-permute-start.12 = (bf16[256,128]{1,0:T(8,128)(2,1)S(1)}, bf16[256,128]{1,0:T(8,128)(2,1)S(1)}, u32[]{:S(2)}, u32[]{:S(2)}) collective-permute-start(bf16[256,128]{1,0:T(8,128)(2,1)S(1)} %get-tuple-element.41), channel_id=1, source_target_pairs={{0,8},{2,10},{4,12},{6,14},{8,0},{10,2},{12,4},{14,6},{1,9},{3,11}... | collective-permute-start | bytes 196616 | tf_op jit(solution)/shard_map/ppermute | solution.py:125
  154.9 6.7 %collective-permute-start.11 = (bf16[256,128]{1,0:T(8,128)(2,1)S(1)}, bf16[256,128]{1,0:T(8,128)(2,1)S(1)}, u32[]{:S(2)}, u32[]{:S(2)}) collective-permute-start(bf16[256,128]{1,0:T(8,128)(2,1)S(1)} %get-tuple-element.39), channel_id=1, source_target_pairs={{0,1},{1,0},{2,3},{3,2},{4,5},{5,4},{6,7},{7,6},{8,9},{9,8},{10,11... | collective-permute-start | bytes 196616 | tf_op jit(solution)/shard_map/ppermute | solution.py:124
